TPU v7x, 32 devices: a whole 2x2x4 slice. The times are simulated.
32 devices in a mesh: sp: 16 (over z, y, x), tp: 2 (over core).
Axes of the slice: x: 2, y: 2, z: 4, core: 2. Of those that a mesh axis runs over, the one named last changes fastest.
Arguments:
- queries: bfloat16 [4096, 1024], P('sp', 'tp'), may hold values from -6 to 6
- keys: bfloat16 [4096, 1024], P('sp', 'tp'), may hold values from -6 to 6
- values: bfloat16 [4096, 1024], P('sp', 'tp'), may hold values from -6 to 6
- lambdas: float32 [8], P('tp'), may hold values from 0.3 to 0.8
- head_gain: float32 [128], replicated, may hold values from 0.1 to 1.9
- out_weight: bfloat16 [1024, 2048], P('tp'), may hold values from -0.1875 to 0.1875
- residual: bfloat16 [4096, 2048], P(('sp', 'tp')), may hold values from -6 to 6
- mix_gain: float32 [2048], replicated, may hold values from 0.1 to 1.9
- pre_gain: float32 [2048], replicated, may hold values from 0.1 to 1.9
- gate_weight: bfloat16 [2048, 2816], P('sp', 'tp'), may hold values from -0.125 to 0.125
- up_weight: bfloat16 [2048, 2816], P('sp', 'tp'), may hold values from -0.125 to 0.125
- down_weight: bfloat16 [2048, 2816], P('sp', 'tp'), may hold values from -0.109375 to 0.109375
- ffn_gain: float32 [2048], replicated, may hold values from 0.1 to 1.9
Outputs:
- result: bfloat16 [4096, 2048], P(('sp', 'tp'))
All inputs are finite; a program needn't handle non-finite values.
Results may differ from a plain program's by a relative error of at most 0.02.
Values may be sent and summed in bfloat16 or wider, within the bound.
A program may use at most 64 MiB of HBM per device.

v0:
```python
import math
import jax
import jax.numpy as jnp
from jax import lax
from jax.sharding import PartitionSpec as P

KD = 64
VD = 128
epsilon = 1e-06
negative = -1e30


def normalize(matrix, gain):
    return matrix * lax.rsqrt(jnp.mean(matrix * matrix, axis=-1, keepdims=True) + epsilon) * gain


def rounded(matrix):
    return lax.optimization_barrier(matrix.astype(jnp.bfloat16)).astype(jnp.float32)


def on_device(
    queries,
    keys,
    values,
    lambdas,
    head_gain,
    out_weight,
    residual,
    mix_gain,
    pre_gain,
    gate_weight,
    up_weight,
    down_weight,
    ffn_gain,
):
    rows = queries.shape[0]
    heads_dev = values.shape[1] // VD
    offset = lax.axis_index("sp") * rows
    scale = 1.0 / math.sqrt(KD)
    groups = [(queries, offset + jnp.arange(rows, dtype=jnp.int32))]
    grids = [
        (group_rows.reshape(group_rows.shape[0], heads_dev, 2, KD), group_pos)
        for group_rows, group_pos in groups
    ]
    initial = tuple(
        (
            (
                jnp.full((heads_dev, 2, grid.shape[0]), negative, jnp.float32),
                jnp.zeros((heads_dev, 2, grid.shape[0]), jnp.float32),
                jnp.zeros((heads_dev, 2, grid.shape[0], VD), jnp.float32),
            )
            for grid, _ in grids
        )
    )
    key_piece = lax.all_gather(keys, "sp", axis=0, tiled=True)
    value_piece = lax.all_gather(values, "sp", axis=0, tiled=True)
    count = key_piece.shape[0]
    block = math.gcd(count, max(256, 2048 // heads_dev))
    key_grid = key_piece.reshape(count, heads_dev, 2, KD)
    value_grid = value_piece.reshape(count, heads_dev, VD)
    results = []
    for (query_grid, query_pos), carried_group in zip(grids, initial):
        last_pos = query_pos[-1]

        def visit(index, carried, query_grid=query_grid, query_pos=query_pos, last_pos=last_pos):
            first = index * block

            def update(current):
                maxima, totals, accum = current
                key_block = lax.dynamic_slice_in_dim(key_grid, first, block, 0)
                value_block = lax.dynamic_slice_in_dim(value_grid, first, block, 0)
                scores = (
                    jnp.einsum(
                        "rhcd,nhcd->hcrn", query_grid, key_block, preferred_element_type=jnp.float32
                    )
                    * scale
                )
                key_pos = first + jnp.arange(block, dtype=jnp.int32)
                visible = key_pos[None, :] <= query_pos[:, None]
                block_max = jnp.max(jnp.where(visible, scores, negative), axis=-1)
                new_max = jnp.maximum(maxima, block_max)
                weights = jnp.where(visible, jnp.exp(scores - new_max[..., None]), 0.0)
                factor = jnp.exp(maxima - new_max)
                totals = totals * factor + jnp.sum(weights, axis=-1)
                accum = accum * factor[..., None] + jnp.einsum(
                    "hcrn,nhe->hcre",
                    weights.astype(jnp.bfloat16),
                    value_block,
                    preferred_element_type=jnp.float32,
                )
                return (new_max, totals, accum)

            return lax.cond(first <= last_pos, update, lambda current: current, carried)

        results.append(lax.fori_loop(0, count // block, visit, carried_group))
    states = tuple(results)
    totals = jnp.concatenate([state[1] for state in states], axis=2)
    accum = jnp.concatenate([state[2] for state in states], axis=2)
    ratio = accum / totals[..., None]
    attended = ratio[:, 0] - lambdas[:, None, None] * ratio[:, 1]
    heads_normed = normalize(attended, head_gain).astype(jnp.bfloat16)
    head_out = jnp.transpose(heads_normed, (1, 0, 2)).reshape(rows, heads_dev * VD)
    section = head_out
    projected = lax.psum_scatter(
        rounded(jnp.dot(section, out_weight, preferred_element_type=jnp.float32)).astype(
            jnp.bfloat16
        ),
        "tp",
        scatter_dimension=0,
        tiled=True,
    ).astype(jnp.float32)
    mixed = (residual.astype(jnp.float32) + normalize(projected, mix_gain)).astype(jnp.bfloat16)
    normed = normalize(mixed.astype(jnp.float32), pre_gain).astype(jnp.bfloat16)
    inputs = lax.all_gather(normed, "tp", axis=0, tiled=True)
    gate_sum = jnp.dot(
        inputs,
        lax.all_gather(gate_weight, "sp", axis=0, tiled=True),
        preferred_element_type=jnp.float32,
    )
    up_sum = jnp.dot(
        inputs,
        lax.all_gather(up_weight, "sp", axis=0, tiled=True),
        preferred_element_type=jnp.float32,
    )
    down_rows = lax.all_gather(down_weight, "sp", axis=0, tiled=True)
    hidden = (jax.nn.silu(gate_sum) * up_sum).astype(jnp.bfloat16)
    section = hidden
    ffn_out = lax.psum_scatter(
        rounded(
            lax.dot_general(
                section, down_rows, (((1,), (1,)), ((), ())), preferred_element_type=jnp.float32
            )
        ).astype(jnp.bfloat16),
        "tp",
        scatter_dimension=0,
        tiled=True,
    ).astype(jnp.float32)
    return (mixed.astype(jnp.float32) + normalize(ffn_out, ffn_gain)).astype(jnp.bfloat16)


def solution(mesh):
    in_specs = (
        P("sp", "tp"),
        P("sp", "tp"),
        P("sp", "tp"),
        P("tp"),
        P(),
        P("tp", None),
        P(("sp", "tp"), None),
        P(),
        P(),
        P("sp", "tp"),
        P("sp", "tp"),
        P("sp", "tp"),
        P(),
    )
    out_specs = P(("sp", "tp"), None)
    return jax.shard_map(
        on_device, mesh=mesh, in_specs=in_specs, out_specs=out_specs, check_vma=False
    )
```

profile of v0, /device:TPU:0, one launch (start us, length us, event | category | flops | bytes accessed | tf_op | source)
XLA Modules:
  0.0 556.5 jit_solution(14109540830264197258)
XLA Ops:
  6.5 0.0 copy-start
  6.5 0.0 all-gather.9.cloned.1.call-start
  6.5 1.9 copy.21
  8.5 0.0 all-gather.9.cloned.1.call-update
  8.5 0.0 all-gather.7.cloned.1.call-start
  8.6 0.7 all-gather.7.cloned.1.call-update
  9.3 0.0 reduce-scatter.3.cloned.1.call-start
  9.3 0.7 slice.9
  10.0 1.1 copy.20
  11.1 88.5 %all-gather.9.cloned.1.call-done = bf16[4096,512]{0,1:T(8,128)(2,1)} async-done(((bf16[256,512]{0,1:T(8,128)(2,1)}), bf16[4096,512]{0,1:T(8,128)(2,1)}) %all-gather.9.cloned.1.call-update) | async-done | bytes 4194320 | tf_op jit(solution)/shard_map/all_gather | solution.py:56
  99.6 6.3 %copy.22 = bf16[4096,4,128]{2,0,1:T(8,128)(2,1)} copy(bf16[4096,4,128]{0,2,1:T(8,128)(2,1)} %bitcast.62) | data formatting | bytes 8388608
  105.9 70.2 %all-gather.7.cloned.1.call-done = bf16[4096,512]{1,0:T(8,128)(2,1)} async-done(((bf16[256,512]{1,0:T(8,128)(2,1)}), bf16[4096,512]{1,0:T(8,128)(2,1)}) %all-gather.7.cloned.1.call-update) | async-done | bytes 4194320 | tf_op jit(solution)/shard_map/all_gather | solution.py:55
  176.2 6.5 %copy.19 = bf16[4096,512]{0,1:T(8,128)(2,1)} copy(bf16[4096,512]{1,0:T(8,128)(2,1)} %all-gather.7.cloned.1.call-done) | data formatting | bytes 8388608 | tf_op jit(solution)/shard_map/all_gather | solution.py:55
  182.7 0.1 broadcast_in_dim.24
  182.8 11.5 %while.18 = (s32[]{:T(128)}, f32[4,2,256]{2,1,0:T(2,128)S(1)}, f32[4,2,256]{2,1,0:T(2,128)S(1)}, f32[4,2,256,128]{3,2,1,0:T(8,128)S(1)}, s32[]{:T(128)}, /*index...) while((s32[]{:T(128)}, f32[4,2,256]{2,1,0:T(2,128)S(1)}, ...), condition=%wide.region_5.6_spmd.clone, body=%wide.region_0.5_spmd.clone.sunk | while | flops 414847744 | bytes 16654649 | solution.py:95
  183.5 5.6 %conditional.3 = ((f32[4,2,256]{2,1,0:T(2,128)S(1)}, f32[4,2,256]{2,1,0:T(2,128)S(1)}, f32[4,2,256,128]{3,2,1,0:T(8,128)S(1)})) conditional(s32[]{:T(128)} %convert_element_type.109, (f32[4,2,256]{2,1,0:T(2,128)S(1)}, f32[4,2,256]{2,1,0:T(2,128)S(1)}, f32[4,2,256,128]{3,2,1,0:T(8,128)S(1)}) %tuple.47, (s32[]{:T(128)}, s32[]{:T(128)}, ...), branch_computations={%region_1.0_spmd, %region_2.4_spmd} | conditional | flops 414847744 | bytes 16653394 | solution.py:93
  183.5 0.1 broadcast_compare_fusion
  183.7 1.9 fusion.2
  185.6 0.9 fusion.6
  186.5 2.6 fusion.13
  194.3 0.0 copy-start.5
  194.3 0.0 copy-start.6
  194.3 1.3 copy.24
  195.6 1.3 broadcast_divide_fusion
  197.0 0.0 copy-done.5
  197.0 0.0 copy-start.1
  197.0 0.0 copy-start.2
  197.0 0.2 multiply_reduce_fusion
  197.1 0.0 copy-start.3
  197.2 0.0 copy-done.6
  197.2 0.1 multiply_convert_fusion
  197.3 0.0 copy-done
  197.4 1.7 convolution_convert_fusion
  199.1 0.0 reduce-scatter.3.cloned.1.call-update
  199.1 0.0 all-gather.13.cloned.1.call-start
  199.1 0.5 all-gather.13.cloned.1.call-update
  199.7 0.0 all-gather.11.cloned.1.call-start
  199.7 45.6 %reduce-scatter.3.cloned.1.call-done = bf16[128,2048]{1,0:T(8,128)(2,1)} async-done(((bf16[256,2048]{1,0:T(8,128)(2,1)}), bf16[128,2048]{1,0:T(8,128)(2,1)}) %reduce-scatter.3.cloned.1.call-update) | async-done | bytes 524304 | tf_op jit(solution)/shard_map/reduce_scatter | solution.py:104
  245.3 1.2 fusion.25
  246.5 0.0 copy-done.1
  246.5 0.0 copy-done.2
  246.6 1.4 fusion.31
  248.0 0.0 copy-done.3
  248.0 1.0 fusion.33
  249.0 0.0 all-gather.11.cloned.1.call-update
  249.0 0.0 all-gather.15.cloned.1.call-start
  249.1 0.5 all-gather.15.cloned.1.call-update
  249.6 0.0 all-gather.17.cloned.1.call-start
  249.7 0.7 all-gather.17.cloned.1.call-update
  250.4 0.0 reduce-scatter.5.cloned.1.call-start
  250.4 87.5 %all-gather.13.cloned.1.call-done = bf16[2048,1408]{1,0:T(8,128)(2,1)} async-done(((bf16[128,1408]{1,0:T(8,128)(2,1)}), bf16[2048,1408]{1,0:T(8,128)(2,1)}) %all-gather.13.cloned.1.call-update) | async-done | bytes 5767184 | tf_op jit(solution)/shard_map/all_gather | solution.py:117
  337.9 9.1 %all-gather.11.cloned.1.call-done = bf16[256,2048]{1,0:T(8,128)(2,1)} async-done(((bf16[128,2048]{1,0:T(8,128)(2,1)}), bf16[256,2048]{1,0:T(8,128)(2,1)}) %all-gather.11.cloned.1.call-update) | async-done | bytes 1048592 | tf_op jit(solution)/shard_map/all_gather | solution.py:114
  347.0 5.9 %fusion.39 = f32[256,1408]{1,0:T(8,128)} fusion(bf16[256,2048]{1,0:T(8,128)(2,1)} %all-gather.11.cloned.1.call-done, bf16[2048,1408]{1,0:T(8,128)(2,1)} %all-gather.13.cloned.1.call-done), kind=kOutput, calls=%fused_computation.61 | convolution fusion | flops 1476395008 | bytes 8257536 | tf_op jit(solution)/shard_map/dot_general | solution.py:115
  352.9 0.0 copy-start.4
  352.9 86.6 %all-gather.15.cloned.1.call-done = bf16[2048,1408]{1,0:T(8,128)(2,1)} async-done(((bf16[128,1408]{1,0:T(8,128)(2,1)}), bf16[2048,1408]{1,0:T(8,128)(2,1)}) %all-gather.15.cloned.1.call-update) | async-done | bytes 5767184 | tf_op jit(solution)/shard_map/all_gather | solution.py:122
  439.5 90.1 %all-gather.17.cloned.1.call-done = bf16[2048,1408]{1,0:T(8,128)(2,1)} async-done(((bf16[128,1408]{1,0:T(8,128)(2,1)}), bf16[2048,1408]{1,0:T(8,128)(2,1)}) %all-gather.17.cloned.1.call-update) | async-done | bytes 5767184 | tf_op jit(solution)/shard_map/all_gather | solution.py:125
  529.6 9.5 %convolution_convert_fusion.1 = bf16[256,2048]{1,0:T(8,128)(2,1)} fusion(bf16[2048,1408]{1,0:T(8,128)(2,1)} %all-gather.17.cloned.1.call-done, bf16[256,2048]{1,0:T(8,128)(2,1)} %all-gather.11.cloned.1.call-done, bf16[2048,1408]{1,0:T(8,128)(2,1)} %all-gather.15.cloned.1.call-done, f32[256,1408]{1,0:T(8,128)} %fusion.39), kind=kOutput, calls=%fused_computation.30 | convolution fusion | flops 2955476992 | bytes 15073280 | tf_op jit(solution)/shard_map/dot_general | solution.py:130
  539.1 0.0 reduce-scatter.5.cloned.1.call-update
  539.1 7.2 %reduce-scatter.5.cloned.1.call-done = bf16[128,2048]{1,0:T(8,128)(2,1)} async-done(((bf16[256,2048]{1,0:T(8,128)(2,1)}), bf16[128,2048]{1,0:T(8,128)(2,1)}) %reduce-scatter.5.cloned.1.call-update) | async-done | bytes 524304 | tf_op jit(solution)/shard_map/reduce_scatter | solution.py:128
  546.3 1.2 fusion.29
  547.6 0.0 copy-done.4
  547.6 2.1 fusion.34
  (28 shorter events, 0.2 us)
Async XLA Ops:
  6.5 190.8 %copy-start = (bf16[512,2048]{1,0:T(8,128)(2,1)S(1)}, bf16[512,2048]{1,0:T(8,128)(2,1)}, u32[]{:S(2)}) copy-start(bf16[512,2048]{1,0:T(8,128)(2,1)} %param.22) | copy-start | bytes 6291460
  6.5 93.0 %all-gather.9.cloned.1.call-start = ((), (), s32[]{:S(2)}) async-start(), calls=%async_computation.3 | async-start | bytes 4456448 | tf_op jit(solution)/shard_map/all_gather | solution.py:56
  8.5 167.7 %all-gather.7.cloned.1.call-start = ((), (), s32[]{:S(2)}) async-start(), calls=%async_computation.2 | async-start | bytes 4456448 | tf_op jit(solution)/shard_map/all_gather | solution.py:55
  9.3 236.0 %reduce-scatter.3.cloned.1.call-start = ((), (), s32[]{:S(2)}) async-start(), calls=%async_computation.4 | async-start | bytes 1572864 | tf_op jit(solution)/shard_map/reduce_scatter | solution.py:104
  194.3 2.7 copy-start.5
  194.3 2.9 copy-start.6
  197.0 49.6 %copy-start.1 = (bf16[128,2048]{1,0:T(8,128)(2,1)S(1)}, bf16[128,2048]{1,0:T(8,128)(2,1)}, u32[]{:S(2)}) copy-start(bf16[128,2048]{1,0:T(8,128)(2,1)} %param.23) | copy-start | bytes 1572868
  197.0 49.6 %copy-start.2 = (f32[2048]{0:T(1024)S(1)}, f32[2048]{0:T(1024)}, u32[]{:S(2)}) copy-start(f32[2048]{0:T(1024)} %param.24) | copy-start | bytes 24580
  197.1 50.9 %copy-start.3 = (f32[2048]{0:T(1024)S(1)}, f32[2048]{0:T(1024)}, u32[]{:S(2)}) copy-start(f32[2048]{0:T(1024)} %param.25) | copy-start | bytes 24580
  199.1 138.8 %all-gather.13.cloned.1.call-start = ((), (), s32[]{:S(2)}) async-start(), calls=%async_computation.6 | async-start | bytes 6127616 | tf_op jit(solution)/shard_map/all_gather | solution.py:117
  199.7 147.3 %all-gather.11.cloned.1.call-start = ((), (), s32[]{:S(2)}) async-start(), calls=%async_computation.5 | async-start | bytes 1572864 | tf_op jit(solution)/shard_map/all_gather | solution.py:114
  249.0 190.5 %all-gather.15.cloned.1.call-start = ((), (), s32[]{:S(2)}) async-start(), calls=%async_computation.7 | async-start | bytes 6127616 | tf_op jit(solution)/shard_map/all_gather | solution.py:122
  249.6 280.0 %all-gather.17.cloned.1.call-start = ((), (), s32[]{:S(2)}) async-start(), calls=%async_computation.8 | async-start | bytes 6127616 | tf_op jit(solution)/shard_map/all_gather | solution.py:125
  250.4 296.0 %reduce-scatter.5.cloned.1.call-start = ((), (), s32[]{:S(2)}) async-start(), calls=%async_computation.9 | async-start | bytes 1572864 | tf_op jit(solution)/shard_map/reduce_scatter | solution.py:128
  352.9 194.7 %copy-start.4 = (f32[2048]{0:T(1024)S(1)}, f32[2048]{0:T(1024)}, u32[]{:S(2)}) copy-start(f32[2048]{0:T(1024)} %param.29) | copy-start | bytes 24580
Sparse Core Ops, SparseCore 0:
  10.1 89.4 all-gather.8
  102.3 73.7 all-gather.6
  199.2 46.0 reduce-scatter.2
  247.8 89.9 all-gather.12
  339.3 7.6 all-gather.10
  349.5 89.9 all-gather.14
  442.2 87.4 all-gather.16
  539.3 7.0 reduce-scatter.4
where the time goes:
time: 558 us; the launch traced here: 557 us
  waiting for transfers between devices  487 us (87%)
  matrix products  21.6 us (4%)
  local copies, waits for them, and re-layouts  18 us (3%)
  between operations  13.7 us (2%)
  other arithmetic  9.68 us (2%)
  loops' own time  5.98 us (1%)
    all_gather x1, waiting for transfers between devices, on_device(): down_rows = lax.all_gather(down_weight, 'sp', axis=0, tiled=True)  90.1 us
    all_gather x1, waiting for transfers between devices, on_device(): value_piece = lax.all_gather(values, 'sp', axis=0, tiled=True)  88.5 us
    all_gather x1, waiting for transfers between devices, on_device(): lax.all_gather(gate_weight, 'sp', axis=0, tiled=True)  87.5 us
    all_gather x1, waiting for transfers between devices, on_device(): lax.all_gather(up_weight, 'sp', axis=0, tiled=True)  86.6 us
    all_gather x1, waiting for transfers between devices, on_device(): key_piece = lax.all_gather(keys, 'sp', axis=0, tiled=True)  70.2 us
    reduce_scatter x1, waiting for transfers between devices, on_device(): lax.psum_scatter(rounded(jnp.dot(section, out_weight, preferred_element_t...  45.6 us
  transfers between devices with their start and end apart: 8, of which 8 were waited for; matrix products, arithmetic and copies ran while one was open for 3% of the time, Pallas kernels for 0%

commit v1 on v0

--- a/solution.py
+++ b/solution.py
@@ -52,8 +52,11 @@
             for grid, _ in grids
         )
     )
-    key_piece = lax.all_gather(keys, "sp", axis=0, tiled=True)
-    value_piece = lax.all_gather(values, "sp", axis=0, tiled=True)
+    key_piece, value_piece = jnp.split(
+        lax.all_gather(jnp.concatenate([keys, values], axis=1), "sp", axis=0, tiled=True),
+        [keys.shape[1]],
+        axis=1,
+    )
     count = key_piece.shape[0]
     block = math.gcd(count, max(256, 2048 // heads_dev))
     key_grid = key_piece.reshape(count, heads_dev, 2, KD)

time: 558 us -> 534 us (0.957)
  waiting for transfers between devices: 487 us -> 463 us
    all_gather x2 -> x1, waiting for transfers between devices: 159 us -> 136 us  [on_device(): lax.all_gather(jnp.concatenate([keys, values], axis=1), 'sp', axis=0, til...]
    all_gather x1 -> x0, local copies, waits for them, and re-layouts: 6.5 us -> none  [on_device(): key_piece = lax.all_gather(keys, 'sp', axis=0, tiled=True)]
    split x0 -> x1, local copies, waits for them, and re-layouts: none -> 5.92 us  [on_device(): jnp.split(lax.all_gather(jnp.concatenate([keys, values], axis=1), 'sp', a...]
  transfers between devices with their start and end apart: 8 -> 7, of which waited for: 8 -> 7; matrix products, arithmetic and copies ran while one was open for 3% -> 2% of each run, Pallas kernels for 0% -> 0%
where the time goes in v1:
time: 534 us; the launch traced here: 532 us
  waiting for transfers between devices  463 us (87%)
  matrix products  21.6 us (4%)
  local copies, waits for them, and re-layouts  17.8 us (3%)
  between operations  13.7 us (3%)
  other arithmetic  10.5 us (2%)
  loops' own time  5.41 us (1%)
    all_gather x1, waiting for transfers between devices, on_device(): lax.all_gather(jnp.concatenate([keys, values], axis=1), 'sp', axis=0, til...  136 us
    all_gather x1, waiting for transfers between devices, on_device(): down_rows = lax.all_gather(down_weight, 'sp', axis=0, tiled=True)  90 us
    all_gather x1, waiting for transfers between devices, on_device(): lax.all_gather(gate_weight, 'sp', axis=0, tiled=True)  87.8 us
    all_gather x1, waiting for transfers between devices, on_device(): lax.all_gather(up_weight, 'sp', axis=0, tiled=True)  86.6 us
    reduce_scatter x1, waiting for transfers between devices, on_device(): lax.psum_scatter(rounded(jnp.dot(section, out_weight, preferred_element_t...  44.9 us
  transfers between devices with their start and end apart: 7, of which 7 were waited for; matrix products, arithmetic and copies ran while one was open for 2% of the time, Pallas kernels for 0%

profile of v1, /device:TPU:0, one launch (start us, length us, event | category | flops | bytes accessed | tf_op | source)
XLA Modules:
  0.0 532.3 jit_solution(8902318351116414442)
XLA Ops:
  6.5 0.0 copy-start
  6.5 0.0 all-gather.6.cloned.1.call-start
  6.5 1.2 copy.19
  7.8 1.1 copy.20
  8.9 0.8 pad_maximum_fusion
  9.7 0.0 all-gather.6.cloned.1.call-update
  9.7 0.0 reduce-scatter.3.cloned.1.call-start
  9.8 0.6 slice.9
  10.4 1.1 copy.21
  11.5 135.8 %all-gather.6.cloned.1.call-done = bf16[4096,1024]{0,1:T(8,128)(2,1)} async-done(((bf16[256,1024]{0,1:T(8,128)(2,1)}), bf16[4096,1024]{0,1:T(8,128)(2,1)}) %all-gather.6.cloned.1.call-update) | async-done | bytes 8388624 | tf_op jit(solution)/shard_map/all_gather | solution.py:56
  147.3 5.9 %fusion.39 = (bf16[4096,512]{0,1:T(8,128)(2,1)}, bf16[4096,512]{0,1:T(8,128)(2,1)}) fusion(bf16[4096,1024]{0,1:T(8,128)(2,1)} %all-gather.6.cloned.1.call-done), kind=kLoop, calls=%fused_computation.62 | loop fusion | bytes 16777216 | tf_op jit(solution)/shard_map/split | solution.py:55
  153.2 6.3 %copy.22 = bf16[4096,4,128]{2,0,1:T(8,128)(2,1)} copy(bf16[4096,4,128]{0,2,1:T(8,128)(2,1)} %bitcast.60) | data formatting | bytes 8388608
  159.6 0.1 broadcast_in_dim.24
  159.7 10.9 %while.18 = (s32[]{:T(128)}, f32[4,2,256]{2,1,0:T(2,128)S(1)}, f32[4,2,256]{2,1,0:T(2,128)S(1)}, f32[4,2,256,128]{3,2,1,0:T(8,128)S(1)}, s32[]{:T(128)}, /*index...) while((s32[]{:T(128)}, f32[4,2,256]{2,1,0:T(2,128)S(1)}, ...), condition=%wide.region_5.6_spmd.clone, body=%wide.region_0.5_spmd.clone.sunk | while | flops 414847744 | bytes 16654649 | solution.py:98
  160.3 5.6 %conditional.3 = ((f32[4,2,256]{2,1,0:T(2,128)S(1)}, f32[4,2,256]{2,1,0:T(2,128)S(1)}, f32[4,2,256,128]{3,2,1,0:T(8,128)S(1)})) conditional(s32[]{:T(128)} %convert_element_type.109, (f32[4,2,256]{2,1,0:T(2,128)S(1)}, f32[4,2,256]{2,1,0:T(2,128)S(1)}, f32[4,2,256,128]{3,2,1,0:T(8,128)S(1)}) %tuple.48, (s32[]{:T(128)}, s32[]{:T(128)}, ...), branch_computations={%region_1.0_spmd, %region_2.4_spmd} | conditional | flops 414847744 | bytes 16653394 | solution.py:96
  160.4 0.1 broadcast_compare_fusion
  160.5 1.9 fusion.2
  162.4 0.9 fusion.6
  163.3 2.6 fusion.13
  170.6 0.0 copy-start.5
  170.6 0.0 copy-start.6
  170.6 1.3 copy.24
  172.0 1.3 broadcast_divide_fusion
  173.3 0.0 copy-done.5
  173.3 0.0 copy-start.1
  173.3 0.0 copy-start.2
  173.3 0.2 multiply_reduce_fusion
  173.5 0.0 copy-start.3
  173.5 0.0 copy-done.6
  173.5 0.1 multiply_convert_fusion
  173.7 0.0 copy-done
  173.7 1.7 convolution_convert_fusion
  175.4 0.0 reduce-scatter.3.cloned.1.call-update
  175.4 0.0 all-gather.10.cloned.1.call-start
  175.5 0.7 all-gather.10.cloned.1.call-update
  176.2 0.0 all-gather.8.cloned.1.call-start
  176.2 44.9 %reduce-scatter.3.cloned.1.call-done = bf16[128,2048]{1,0:T(8,128)(2,1)} async-done(((bf16[256,2048]{1,0:T(8,128)(2,1)}), bf16[128,2048]{1,0:T(8,128)(2,1)}) %reduce-scatter.3.cloned.1.call-update) | async-done | bytes 524304 | tf_op jit(solution)/shard_map/reduce_scatter | solution.py:107
  221.1 1.2 fusion.25
  222.3 0.0 copy-done.1
  222.3 0.0 copy-done.2
  222.3 1.4 fusion.31
  223.8 0.0 copy-done.3
  223.8 1.0 fusion.33
  224.8 0.0 all-gather.8.cloned.1.call-update
  224.8 0.0 all-gather.12.cloned.1.call-start
  224.9 0.5 all-gather.12.cloned.1.call-update
  225.4 0.0 all-gather.14.cloned.1.call-start
  225.5 0.5 all-gather.14.cloned.1.call-update
  226.0 0.0 reduce-scatter.5.cloned.1.call-start
  226.0 87.8 %all-gather.10.cloned.1.call-done = bf16[2048,1408]{1,0:T(8,128)(2,1)} async-done(((bf16[128,1408]{1,0:T(8,128)(2,1)}), bf16[2048,1408]{1,0:T(8,128)(2,1)}) %all-gather.10.cloned.1.call-update) | async-done | bytes 5767184 | tf_op jit(solution)/shard_map/all_gather | solution.py:120
  313.8 9.1 %all-gather.8.cloned.1.call-done = bf16[256,2048]{1,0:T(8,128)(2,1)} async-done(((bf16[128,2048]{1,0:T(8,128)(2,1)}), bf16[256,2048]{1,0:T(8,128)(2,1)}) %all-gather.8.cloned.1.call-update) | async-done | bytes 1048592 | tf_op jit(solution)/shard_map/all_gather | solution.py:117
  322.9 5.9 %fusion.40 = f32[256,1408]{1,0:T(8,128)} fusion(bf16[256,2048]{1,0:T(8,128)(2,1)} %all-gather.8.cloned.1.call-done, bf16[2048,1408]{1,0:T(8,128)(2,1)} %all-gather.10.cloned.1.call-done), kind=kOutput, calls=%fused_computation.63 | convolution fusion | flops 1476395008 | bytes 8257536 | tf_op jit(solution)/shard_map/dot_general | solution.py:118
  328.8 0.0 copy-start.4
  328.8 86.6 %all-gather.12.cloned.1.call-done = bf16[2048,1408]{1,0:T(8,128)(2,1)} async-done(((bf16[128,1408]{1,0:T(8,128)(2,1)}), bf16[2048,1408]{1,0:T(8,128)(2,1)}) %all-gather.12.cloned.1.call-update) | async-done | bytes 5767184 | tf_op jit(solution)/shard_map/all_gather | solution.py:125
  415.4 90.0 %all-gather.14.cloned.1.call-done = bf16[2048,1408]{1,0:T(8,128)(2,1)} async-done(((bf16[128,1408]{1,0:T(8,128)(2,1)}), bf16[2048,1408]{1,0:T(8,128)(2,1)}) %all-gather.14.cloned.1.call-update) | async-done | bytes 5767184 | tf_op jit(solution)/shard_map/all_gather | solution.py:128
  505.4 9.5 %convolution_convert_fusion.1 = bf16[256,2048]{1,0:T(8,128)(2,1)} fusion(bf16[2048,1408]{1,0:T(8,128)(2,1)} %all-gather.14.cloned.1.call-done, bf16[256,2048]{1,0:T(8,128)(2,1)} %all-gather.8.cloned.1.call-done, bf16[2048,1408]{1,0:T(8,128)(2,1)} %all-gather.12.cloned.1.call-done, f32[256,1408]{1,0:T(8,128)} %fusion.40), kind=kOutput, calls=%fused_computation.30 | convolution fusion | flops 2955476992 | bytes 15073280 | tf_op jit(solution)/shard_map/dot_general | solution.py:133
  514.9 0.0 reduce-scatter.5.cloned.1.call-update
  514.9 7.2 %reduce-scatter.5.cloned.1.call-done = bf16[128,2048]{1,0:T(8,128)(2,1)} async-done(((bf16[256,2048]{1,0:T(8,128)(2,1)}), bf16[128,2048]{1,0:T(8,128)(2,1)}) %reduce-scatter.5.cloned.1.call-update) | async-done | bytes 524304 | tf_op jit(solution)/shard_map/reduce_scatter | solution.py:131
  522.1 1.2 fusion.29
  523.4 0.0 copy-done.4
  523.4 2.1 fusion.34
  (28 shorter events, 0.2 us)
Async XLA Ops:
  6.5 167.1 %copy-start = (bf16[512,2048]{1,0:T(8,128)(2,1)S(1)}, bf16[512,2048]{1,0:T(8,128)(2,1)}, u32[]{:S(2)}) copy-start(bf16[512,2048]{1,0:T(8,128)(2,1)} %param.22) | copy-start | bytes 6291460
  6.5 140.8 %all-gather.6.cloned.1.call-start = ((), (), s32[]{:S(2)}) async-start(), calls=%async_computation.2 | async-start | bytes 8912896 | tf_op jit(solution)/shard_map/all_gather | solution.py:56
  9.7 211.4 %reduce-scatter.3.cloned.1.call-start = ((), (), s32[]{:S(2)}) async-start(), calls=%async_computation.3 | async-start | bytes 1572864 | tf_op jit(solution)/shard_map/reduce_scatter | solution.py:107
  170.6 2.7 copy-start.5
  170.6 2.9 copy-start.6
  173.3 49.0 %copy-start.1 = (bf16[128,2048]{1,0:T(8,128)(2,1)S(1)}, bf16[128,2048]{1,0:T(8,128)(2,1)}, u32[]{:S(2)}) copy-start(bf16[128,2048]{1,0:T(8,128)(2,1)} %param.23) | copy-start | bytes 1572868
  173.3 49.0 %copy-start.2 = (f32[2048]{0:T(1024)S(1)}, f32[2048]{0:T(1024)}, u32[]{:S(2)}) copy-start(f32[2048]{0:T(1024)} %param.24) | copy-start | bytes 24580
  173.5 50.3 %copy-start.3 = (f32[2048]{0:T(1024)S(1)}, f32[2048]{0:T(1024)}, u32[]{:S(2)}) copy-start(f32[2048]{0:T(1024)} %param.25) | copy-start | bytes 24580
  175.4 138.4 %all-gather.10.cloned.1.call-start = ((), (), s32[]{:S(2)}) async-start(), calls=%async_computation.5 | async-start | bytes 6127616 | tf_op jit(solution)/shard_map/all_gather | solution.py:120
  176.2 146.7 %all-gather.8.cloned.1.call-start = ((), (), s32[]{:S(2)}) async-start(), calls=%async_computation.4 | async-start | bytes 1572864 | tf_op jit(solution)/shard_map/all_gather | solution.py:117
  224.8 190.6 %all-gather.12.cloned.1.call-start = ((), (), s32[]{:S(2)}) async-start(), calls=%async_computation.6 | async-start | bytes 6127616 | tf_op jit(solution)/shard_map/all_gather | solution.py:125
  225.4 280.0 %all-gather.14.cloned.1.call-start = ((), (), s32[]{:S(2)}) async-start(), calls=%async_computation.7 | async-start | bytes 6127616 | tf_op jit(solution)/shard_map/all_gather | solution.py:128
  226.0 296.1 %reduce-scatter.5.cloned.1.call-start = ((), (), s32[]{:S(2)}) async-start(), calls=%async_computation.8 | async-start | bytes 1572864 | tf_op jit(solution)/shard_map/reduce_scatter | solution.py:131
  328.8 194.5 %copy-start.4 = (f32[2048]{0:T(1024)S(1)}, f32[2048]{0:T(1024)}, u32[]{:S(2)}) copy-start(f32[2048]{0:T(1024)} %param.29) | copy-start | bytes 24580
Sparse Core Ops, SparseCore 0:
  10.1 137.1 all-gather.5
  175.6 45.4 reduce-scatter.2
  223.8 89.9 all-gather.9
  315.2 7.6 all-gather.7
  325.5 89.9 all-gather.11
  418.0 87.4 all-gather.13
  515.0 7.0 reduce-scatter.4
